TPU v7x, 32 devices: a whole 2x2x4 slice. The times are simulated.
32 devices in a mesh: dp: 4 (over y, x), kv: 4 (over z), tp: 2 (over core).
Axes of the slice: x: 2, y: 2, z: 4, core: 2. Of those that a mesh axis runs over, the one named last changes fastest.
Arguments:
- tokens: bfloat16 [32, 2048], P('dp', ('kv', 'tp')), as said below
- first_gain: float32 [2048], replicated, may hold values from 0.1 to 1.9
- first_gate: bfloat16 [2048, 5632], P(None, ('kv', 'tp')), may hold values from -0.125 to 0.125
- first_up: bfloat16 [2048, 5632], P(None, ('kv', 'tp')), may hold values from -0.125 to 0.125
- first_down: bfloat16 [5632, 2048], P(('kv', 'tp')), may hold values from -0.109375 to 0.109375
- mix_gain: float32 [2048], P(('kv', 'tp')), may hold values from 0.1 to 1.9
- w_input: bfloat16 [2048, 2048], P(('kv', 'tp')), may hold values from -0.125 to 0.125
- w_outgate: bfloat16 [2048, 2048], P(('kv', 'tp')), may hold values from -0.125 to 0.125
- w_write: bfloat16 [2048, 512], P(('kv', 'tp')), may hold values from -0.125 to 0.125
- w_read: bfloat16 [2048, 512], P(('kv', 'tp')), may hold values from -0.125 to 0.125
- w_step: bfloat16 [2048, 32], P(('kv', 'tp')), may hold values from -0.125 to 0.125
- conv_taps: bfloat16 [4, 3072], replicated, may hold values from -3 to 3
- conv_history: bfloat16 [32, 3, 3072], P(('dp', 'kv', 'tp')), may hold values from -6 to 6
- step_bias: float32 [32], replicated, may hold values from -6 to -1
- rate_log: float32 [32], replicated, may hold values from 0 to 2.77
- mixer_state: float32 [32, 32, 64, 128], P(('dp', 'kv', 'tp')), may hold values from -4 to 4
- group_gain: float32 [2048], replicated, may hold values from 0.1 to 1.9
- w_output: bfloat16 [2048, 2048], P(None, ('kv', 'tp')), may hold values from -0.125 to 0.125
- second_gain: float32 [2048], replicated, may hold values from 0.1 to 1.9
- second_gate: bfloat16 [2048, 5632], P(None, ('kv', 'tp')), may hold values from -0.125 to 0.125
- second_up: bfloat16 [2048, 5632], P(None, ('kv', 'tp')), may hold values from -0.125 to 0.125
- second_down: bfloat16 [5632, 2048], P(('kv', 'tp')), may hold values from -0.109375 to 0.109375
Outputs:
- layer_out: bfloat16 [32, 2048], P('dp', ('kv', 'tp'))
- state_out: float32 [32, 32, 64, 128], P(('dp', 'kv', 'tp'))
- history_out: bfloat16 [32, 3, 3072], P(('dp', 'kv', 'tp'))
Inputs may be any that keep to these rules, and one draw needn't show every extreme that they name: `tokens`: channel scales rise along the width.
All inputs are finite; a program needn't handle non-finite values.
Results may differ from a plain program's by a relative error of at most 0.014.
Values may be sent and summed in bfloat16 or wider, within the bound.
A program may use at most 64 MiB of HBM per device.

v0:
```python
import jax
import jax.numpy as jnp
from jax import lax
from jax.sharding import PartitionSpec as P

EPS = 1e-06


def half_block(resid, gain, w_gate, w_up, w_down):
    whole = lax.all_gather(resid, ("kv", "tp"), axis=1, tiled=True)
    whole_f = whole.astype(jnp.float32)
    scale = lax.rsqrt(jnp.mean(whole_f * whole_f, axis=-1, keepdims=True) + EPS)
    normed = (whole_f * scale * gain).astype(jnp.bfloat16)
    gate = jnp.dot(normed, w_gate, preferred_element_type=jnp.float32)
    upper = jnp.dot(normed, w_up, preferred_element_type=jnp.float32)
    hidden = (jax.nn.silu(gate) * upper).astype(jnp.bfloat16)
    down = jnp.dot(hidden, w_down, preferred_element_type=jnp.float32)
    share = lax.psum_scatter(down, ("kv", "tp"), scatter_dimension=1, tiled=True)
    return (resid.astype(jnp.float32) + 0.5 * share).astype(jnp.bfloat16)


def body(
    tokens,
    first_gain,
    first_gate,
    first_up,
    first_down,
    mix_gain,
    w_input,
    w_outgate,
    w_write,
    w_read,
    w_step,
    conv_taps,
    conv_history,
    step_bias,
    rate_log,
    mixer_state,
    group_gain,
    w_output,
    second_gain,
    second_gate,
    second_up,
    second_down,
):
    width = first_gate.shape[0]
    count = mixer_state.shape[0]
    heads = mixer_state.shape[1]
    head_dim = mixer_state.shape[2]
    state_dim = mixer_state.shape[3]
    ssd_width = heads * head_dim
    groups = w_write.shape[1] // state_dim
    per_group = heads // groups
    first = half_block(tokens, first_gain, first_gate, first_up, first_down)
    first_f = first.astype(jnp.float32)
    squares = jnp.sum(first_f * first_f, axis=1)
    premix = (first_f * mix_gain).astype(jnp.bfloat16)
    part_input = jnp.dot(premix, w_input, preferred_element_type=jnp.float32)
    part_write = jnp.dot(premix, w_write, preferred_element_type=jnp.float32)
    part_read = jnp.dot(premix, w_read, preferred_element_type=jnp.float32)
    part_step = jnp.dot(premix, w_step, preferred_element_type=jnp.float32)
    part_gate = jnp.dot(premix, w_outgate, preferred_element_type=jnp.float32)
    totals = lax.psum(squares, ("kv", "tp"))
    head_terms = (part_input, part_write, part_read, part_step)
    extra_terms = ()
    summed = lax.psum_scatter(
        head_terms + extra_terms + (part_gate,), ("kv", "tp"), scatter_dimension=0, tiled=True
    )
    gate_sum = summed[-1]
    summed = summed[:-1]
    own_squares = lax.dynamic_slice_in_dim(totals, lax.axis_index(("kv", "tp")) * count, count, 0)
    scale = lax.rsqrt(own_squares / width + EPS)[:, None]
    inputs = (scale * summed[0]).astype(jnp.bfloat16)
    writes = (scale * summed[1]).astype(jnp.bfloat16)
    reads = (scale * summed[2]).astype(jnp.bfloat16)
    steps_raw = (scale * summed[3]).astype(jnp.bfloat16)
    fresh = jnp.concatenate([inputs, writes, reads], axis=1)
    window = jnp.concatenate([conv_history, fresh[:, None, :]], axis=1)
    history_out = window[:, 1:]
    conv = jax.nn.silu(
        jnp.sum(window.astype(jnp.float32) * conv_taps.astype(jnp.float32)[None], axis=1)
    )
    conv_in = conv[:, :ssd_width].reshape(count, groups, per_group, head_dim)
    conv_write = conv[:, ssd_width : ssd_width + groups * state_dim].reshape(
        count, groups, state_dim
    )
    conv_read = conv[:, ssd_width + groups * state_dim :].reshape(count, groups, state_dim)
    step = jax.nn.softplus(steps_raw.astype(jnp.float32) + step_bias)
    decay = jnp.exp(-step * jnp.exp(rate_log))
    state = mixer_state.reshape(count, groups, per_group, head_dim, state_dim)
    decay_g = decay.reshape(count, groups, per_group)
    step_g = step.reshape(count, groups, per_group)
    written = (step_g[..., None] * conv_in)[..., None] * conv_write[:, :, None, None, :]
    new_state = decay_g[..., None, None] * state + written
    read_out = jnp.einsum("sgjpn,sgn->sgjp", new_state, conv_read, precision=lax.Precision.HIGHEST)
    outgate = (scale * gate_sum).astype(jnp.bfloat16)
    gated = read_out.reshape(count, ssd_width) * jax.nn.silu(outgate.astype(jnp.float32))
    blocks = gated.reshape(count, groups, ssd_width // groups)
    block_scale = lax.rsqrt(jnp.mean(blocks * blocks, axis=-1, keepdims=True) + EPS)
    normed = ((blocks * block_scale).reshape(count, ssd_width) * group_gain).astype(jnp.bfloat16)
    mixed = jnp.dot(
        lax.all_gather(normed, ("kv", "tp"), axis=0, tiled=True),
        w_output,
        preferred_element_type=jnp.float32,
    )
    second = (first_f + mixed).astype(jnp.bfloat16)
    layer_out = half_block(second, second_gain, second_gate, second_up, second_down)
    state_out = new_state.reshape(count, heads, head_dim, state_dim)
    return (layer_out, state_out, history_out)


def solution(mesh):
    return jax.shard_map(
        body,
        mesh=mesh,
        in_specs=(
            P("dp", ("kv", "tp")),
            P(),
            P(None, ("kv", "tp")),
            P(None, ("kv", "tp")),
            P(("kv", "tp"), None),
            P(("kv", "tp")),
            P(("kv", "tp"), None),
            P(("kv", "tp"), None),
            P(("kv", "tp"), None),
            P(("kv", "tp"), None),
            P(("kv", "tp"), None),
            P(),
            P(("dp", "kv", "tp"), None, None),
            P(),
            P(),
            P(("dp", "kv", "tp"), None, None, None),
            P(),
            P(None, ("kv", "tp")),
            P(),
            P(None, ("kv", "tp")),
            P(None, ("kv", "tp")),
            P(("kv", "tp"), None),
        ),
        out_specs=(
            P("dp", ("kv", "tp")),
            P(("dp", "kv", "tp"), None, None, None),
            P(("dp", "kv", "tp"), None, None),
        ),
        check_vma=False,
    )
```

profile of v0, /device:TPU:0, one launch (start us, length us, event | category | flops | bytes accessed | tf_op | source)
XLA Modules:
  0.0 234.0 jit_solution(7709291567706687449)
XLA Ops:
  7.2 16.1 %all_gather.9 = bf16[8,2048]{1,0:T(8,128)(2,1)S(1)} all-gather(bf16[8,256]{1,0:T(8,128)(2,1)} %param.22), channel_id=1, replica_groups=mesh['dp'=4,'kv'=4,'tp'=2] {'kv','tp'}, dimensions={1}, use_global_device_ids=true | all-gather | bytes 36864 | tf_op jit(solution)/shard_map/all_gather | solution.py:10
  23.4 2.7 %fusion.42 = f32[8,704]{1,0:T(8,128)S(1)} fusion(bf16[2048,704]{0,1:T(8,128)(2,1)} %param.24, bf16[8,2048]{1,0:T(8,128)(2,1)S(1)} %all_gather.9, f32[2048]{0:T(1024)} %param.23, f32[8]{0:T(128)S(1)} %add_rsqrt_fusion.2), kind=kOutput, calls=%fused_computation.61 | convolution fusion | flops 23134208 | bytes 2947104 | tf_op jit(solution)/shard_map/dot_general | solution.py:14
  26.2 4.2 %fusion.3 = f32[8,2048]{1,0:T(8,128)} fusion(bf16[704,2048]{1,0:T(8,128)(2,1)S(1)} %copy-done, bf16[2048,704]{0,1:T(8,128)(2,1)} %param.25, f32[8,704]{1,0:T(8,128)S(1)} %fusion.42, bf16[8,2048]{1,0:T(8,128)(2,1)S(1)} %all_gather.9, f32[2048]{0:T(1024)S(1)} %copy-done.4, f32[8]{0:T(128)S(1)} %add_rsqrt_fusion.2), kind=kOutput, calls=%fused_computation.5 | convolution fusion | flops 46236672 | bytes 5896224 | tf_op jit(solution)/shard_map/dot_general | solution.py:17
  31.1 31.0 %reduce-scatter.3.cloned.1.call-done = f32[8,256]{1,0:T(8,128)} async-done(((f32[8,2048]{1,0:T(8,128)}), f32[8,256]{1,0:T(8,128)}) %reduce-scatter.3.cloned.1.call-update) | async-done | bytes 8208 | tf_op jit(solution)/shard_map/reduce_scatter | solution.py:18
  62.0 0.8 fusion.31
  63.3 26.4 %all-reduce.5 = (f32[8,512]{1,0:T(8,128)S(1)}, f32[8]{0:T(128)S(1)}, f32[8,512]{1,0:T(8,128)S(1)}, f32[8,32]{1,0:T(8,128)S(1)}) all-reduce(f32[8,512]{1,0:T(8,128)S(1)} %fusion.53, f32[8]{0:T(128)S(1)} %get-tuple-element.14, f32[8,512]{1,0:T(8,128)S(1)} %fusion.55, ...), channel_id=7, replica_groups=mesh['dp'=4,'kv'=4,'tp'=2] {'kv','tp'}, use_global_device_ids=true, to_apply=%region_7.8.clone | all-reduce | flops 8456 | bytes 67648
  91.0 2.1 fusion.57
  93.1 2.1 fusion.51
  95.7 1.3 fusion.64
  97.0 0.6 reduce.20
  97.9 0.7 fusion.44
  98.6 52.9 %all-reduce.9.cloned.1.call-done = (f32[8,2048]{1,0:T(8,128)}, f32[8,2048]{1,0:T(8,128)}) async-done(((f32[8,2048]{1,0:T(8,128)}, f32[8,2048]{1,0:T(8,128)}), (f32[8,2048]{1,0:T(8,128)}, f32[8,2048]{1,0:T(8,128)})) %all-reduce.9.cloned.1.call-update) | async-done | bytes 131088
  151.5 1.5 fusion.35
  153.3 3.8 %fusion.5 = f32[4,1,8,64]{3,1,2,0:T(1,128)S(1)} fusion(f32[4,8,64,128]{3,2,1,0:T(8,128)} %bitcast.47, f32[4,128]{1,0:T(4,128)S(1)} %bitcast.55, f32[4,8,64]{2,1,0:T(8,128)S(1)} %broadcast_multiply_fusion.1, f32[4,8]{1,0:T(4,128)S(1)} %mul.263, f32[1,3072]{1,0:T(1,128)S(1)} %divide_multiply_fusion), kind=kOutput, calls=%fused_computation.9 | convolution fusion | flops 3932160 | bytes 1079296 | tf_op jit(solution)/shard_map/sgjpn,sgn->sgjp/dot_general | solution.py:95
  157.2 1.6 multiply_reduce_fusion.1
  159.0 14.1 %all-gather = bf16[16384]{0:T(1024)(128)(2,1)S(1)} all-gather(bf16[2048]{0:T(1024)(128)(2,1)S(1)} %multiply_convert_fusion), channel_id=2, replica_groups=mesh['dp'=4,'kv'=4,'tp'=2] {'kv','tp'}, dimensions={0}, use_global_device_ids=true | all-gather | bytes 36864 | tf_op jit(solution)/shard_map/all_gather | solution.py:102
  173.1 1.5 fusion.4
  174.6 14.1 %all_gather.11 = bf16[8,2048]{1,0:T(8,128)(2,1)S(1)} all-gather(bf16[8,256]{1,0:T(8,128)(2,1)S(1)} %fusion.4), channel_id=1, replica_groups=mesh['dp'=4,'kv'=4,'tp'=2] {'kv','tp'}, dimensions={1}, use_global_device_ids=true | all-gather | bytes 36864 | tf_op jit(solution)/shard_map/all_gather | solution.py:10
  188.8 2.7 %fusion.38 = f32[8,704]{1,0:T(8,128)S(1)} fusion(bf16[2048,704]{0,1:T(8,128)(2,1)} %param.41, bf16[8,2048]{1,0:T(8,128)(2,1)S(1)} %all_gather.11, f32[2048]{0:T(1024)S(1)} %copy-done.5, f32[8]{0:T(128)S(1)} %add_rsqrt_fusion), kind=kOutput, calls=%fused_computation.60 | convolution fusion | flops 23134208 | bytes 2947104 | tf_op jit(solution)/shard_map/dot_general | solution.py:14
  191.5 5.0 %fusion.2 = f32[8,2048]{1,0:T(8,128)} fusion(bf16[704,2048]{1,0:T(8,128)(2,1)} %param.43, bf16[2048,704]{0,1:T(8,128)(2,1)} %param.42, f32[8,704]{1,0:T(8,128)S(1)} %fusion.38, bf16[8,2048]{1,0:T(8,128)(2,1)S(1)} %all_gather.11, f32[2048]{0:T(1024)S(1)} %copy-done.5, f32[8]{0:T(128)S(1)} %add_rsqrt_fusion), kind=kOutput, calls=%fused_computation.4 | convolution fusion | flops 46236672 | bytes 5896224 | tf_op jit(solution)/shard_map/dot_general | solution.py:17
  196.6 0.6 pad_maximum_fusion
  197.3 2.6 %multiply_add_fusion = f32[1,32,64,128]{3,2,1,0:T(8,128)} fusion(f32[1,32,64,128]{3,2,1,0:T(8,128)} %param.37, f32[32,128]{1,0:T(8,128)S(1)} %broadcast_bitcast_fusion, f32[32,64]{1,0:T(8,128)S(1)} %broadcast_multiply_fusion, f32[32]{0:T(128)S(1)} %bitcast.56), kind=kLoop, calls=%fused_computation.8 | loop fusion | flops 786432 | bytes 2121856 | tf_op jit(solution)/shard_map/add | solution.py:94
  199.9 26.3 %reduce-scatter.5.cloned.1.call-done = f32[8,256]{1,0:T(8,128)} async-done(((f32[8,2048]{1,0:T(8,128)}), f32[8,256]{1,0:T(8,128)}) %reduce-scatter.5.cloned.1.call-update) | async-done | bytes 8208 | tf_op jit(solution)/shard_map/reduce_scatter | solution.py:18
  226.2 1.3 add_convert_fusion
  (63 shorter events, 3.6 us)
Async XLA Ops:
  7.2 19.0 %copy-start = (bf16[704,2048]{1,0:T(8,128)(2,1)S(1)}, bf16[704,2048]{1,0:T(8,128)(2,1)}, u32[]{:S(2)}) copy-start(bf16[704,2048]{1,0:T(8,128)(2,1)} %param.26) | copy-start | bytes 8650756
  7.2 18.9 %copy-start.4 = (f32[2048]{0:T(1024)S(1)}, f32[2048]{0:T(1024)}, u32[]{:S(2)}) copy-start(f32[2048]{0:T(1024)} %param.23) | copy-start | bytes 24580
  7.2 54.9 %reduce-scatter.3.cloned.1.call-start = ((), (), s32[]{:S(2)}) async-start(), calls=%async_computation.2 | async-start | bytes 73728 | tf_op jit(solution)/shard_map/reduce_scatter | solution.py:18
  26.1 4.4 %copy-start.13 = (u32[32]{0:T(128)S(1)}, u32[32]{0:T(128)}, u32[]{:S(2)}) copy-start(u32[32]{0:T(128)} %constant.47) | copy-start | bytes 388
  26.1 35.9 %copy-start.9 = (bf16[8,256]{1,0:T(8,128)(2,1)S(1)}, bf16[8,256]{1,0:T(8,128)(2,1)}, u32[]{:S(2)}) copy-start(bf16[8,256]{1,0:T(8,128)(2,1)} %param.22) | copy-start | bytes 12292
  26.2 36.7 %copy-start.1 = (bf16[256,512]{1,0:T(8,128)(2,1)S(1)}, bf16[256,512]{1,0:T(8,128)(2,1)}, u32[]{:S(2)}) copy-start(bf16[256,512]{1,0:T(8,128)(2,1)} %param.31) | copy-start | bytes 786436
  26.2 36.7 %copy-start.6 = (f32[256]{0:T(256)S(1)}, f32[256]{0:T(256)}, u32[]{:S(2)}) copy-start(f32[256]{0:T(256)} %param.27) | copy-start | bytes 3076
  26.2 36.8 %copy-start.2 = (bf16[256,512]{1,0:T(8,128)(2,1)S(1)}, bf16[256,512]{1,0:T(8,128)(2,1)}, u32[]{:S(2)}) copy-start(bf16[256,512]{1,0:T(8,128)(2,1)} %param.30) | copy-start | bytes 786436
  26.2 37.0 %copy-start.8 = (bf16[256,32]{0,1:T(8,128)(2,1)S(1)}, bf16[256,32]{0,1:T(8,128)(2,1)}, u32[]{:S(2)}) copy-start(bf16[256,32]{0,1:T(8,128)(2,1)} %param.32) | copy-start | bytes 49156
  30.4 65.4 %copy-start.11 = (f32[32]{0:T(128)S(1)}, f32[32]{0:T(128)}, u32[]{:S(2)}) copy-start(f32[32]{0:T(128)} %param.36) | copy-start | bytes 388
  30.4 65.4 %copy-start.12 = (f32[32]{0:T(128)S(1)}, f32[32]{0:T(128)}, u32[]{:S(2)}) copy-start(f32[32]{0:T(128)} %param.35) | copy-start | bytes 388
  30.4 122.6 %copy-start.3 = (bf16[1,3,3072]{2,1,0:T(4,128)(2,1)S(1)}, bf16[1,3,3072]{2,1,0:T(4,128)(2,1)}, u32[]{:S(2)}) copy-start(bf16[1,3,3072]{2,1,0:T(4,128)(2,1)} %param.34) | copy-start | bytes 55300
  30.4 122.6 %copy-start.7 = (bf16[4,3072]{1,0:T(4,128)(2,1)S(1)}, bf16[4,3072]{1,0:T(4,128)(2,1)}, u32[]{:S(2)}) copy-start(bf16[4,3072]{1,0:T(4,128)(2,1)} %param.33) | copy-start | bytes 73732
  30.4 128.6 %copy-start.10 = (f32[2048]{0:T(1024)S(1)}, f32[2048]{0:T(1024)}, u32[]{:S(2)}) copy-start(f32[2048]{0:T(1024)} %param.38) | copy-start | bytes 24580
  30.4 121.1 %all-reduce.9.cloned.1.call-start = ((), (), s32[]{:S(2)}) async-start(), calls=%async_computation.4 | async-start | bytes 262144
  62.9 126.0 %copy-start.5 = (f32[2048]{0:T(1024)S(1)}, f32[2048]{0:T(1024)}, u32[]{:S(2)}) copy-start(f32[2048]{0:T(1024)} %param.40) | copy-start | bytes 24580
  97.9 128.3 %reduce-scatter.5.cloned.1.call-start = ((), (), s32[]{:S(2)}) async-start(), calls=%async_computation.3 | async-start | bytes 73728 | tf_op jit(solution)/shard_map/reduce_scatter | solution.py:18
Sparse Core Ops, SparseCore 0:
  30.5 31.4 reduce-scatter.2
  98.0 53.4 all-reduce.8
  196.6 29.4 reduce-scatter.4
where the time goes:
time: 235 us; the launch traced here: 234 us
  waiting for transfers between devices  110 us (47%)
  blocking collectives  70.6 us (30%)
  matrix products  24.4 us (10%)
  between operations  14.7 us (6%)
  other arithmetic  11.7 us (5%)
    reduce_scatter x2, waiting for transfers between devices, half_block(): lax.psum_scatter(down, ('kv', 'tp'), scatter_dimension=1, tiled=True)  57.2 us
    unnamed x4, waiting for transfers between devices  53 us
    all_gather x2, blocking collectives, half_block(): whole = lax.all_gather(resid, ('kv', 'tp'), axis=1, tiled=True)  30.1 us
    unnamed x1, blocking collectives  26.4 us
    all_gather x1, blocking collectives, body(): lax.all_gather(normed, ('kv', 'tp'), axis=0, tiled=True)  14.1 us
    dot_general x2, matrix products, half_block(): down = jnp.dot(hidden, w_down, preferred_element_type=jnp.float32)  9.15 us
    dot_general x2, matrix products, half_block(): gate = jnp.dot(normed, w_gate, preferred_element_type=jnp.float32)  5.33 us
  transfers between devices with their start and end apart: 3, of which 3 were waited for; matrix products, arithmetic and copies ran while one was open for 2% of the time, Pallas kernels for 0%

commit v1 on v0

--- a/solution.py
+++ b/solution.py
@@ -1,12 +1,535 @@
+import functools
+import math
+
 import jax
 import jax.numpy as jnp
 from jax import lax
+from jax.experimental import pallas as pl
+from jax.experimental.pallas import tpu as pltpu
 from jax.sharding import PartitionSpec as P
 
 EPS = 1e-06
-
-
-def half_block(resid, gain, w_gate, w_up, w_down):
+F32 = jnp.float32
+BF16 = jnp.bfloat16
+LANES = 128
+VMEM_BYTES = 67043328
+MESH = pl.DeviceIdType.MESH
+
+
+def silu(x):
+    return x * jax.nn.sigmoid(x)
+
+
+def dot_rows(left, right):
+    contract = (((1,), (1,)), ((), ()))
+    return lax.dot_general(left, right, contract, preferred_element_type=F32)
+
+
+def layer_kernel(
+    kv,
+    tp,
+    heads,
+    tokens,
+    first_gain,
+    first_gate,
+    first_up,
+    first_down,
+    mix_gain,
+    w_input,
+    w_outgate,
+    w_write,
+    w_read,
+    w_step,
+    conv_taps,
+    conv_history,
+    step_bias,
+    rate_log,
+    mixer_state,
+    group_gain,
+    w_output,
+    second_gain,
+    second_gate,
+    second_up,
+    second_down,
+    layer_out,
+    state_out,
+    history_out,
+    g1,
+    wg1,
+    wu1,
+    wd1,
+    mg,
+    wi,
+    wo,
+    ww,
+    wr,
+    ws,
+    taps,
+    hist,
+    bias,
+    rate,
+    state,
+    ggain,
+    wout,
+    g2,
+    wg2,
+    wu2,
+    wd2,
+    tok_all,
+    down_send1,
+    down_recv1,
+    proj_send,
+    proj_recv,
+    norm_all,
+    sec_all,
+    down_send2,
+    down_recv2,
+    proj_f,
+    step_f,
+    state_b,
+    hist_f,
+    taps_f,
+    fresh_f,
+    dots_f,
+    tail_f,
+    norm_f,
+    load_sem,
+    send_sem,
+    recv_sem,
+):
+    n = kv * tp
+    rows, chan = tokens.shape
+    width = n * chan
+    rows_in = w_input.shape[1] // LANES
+    rows_map = w_write.shape[1] // LANES
+    rows_conv = rows_in + 2 * rows_map
+    rows_all = rows_conv + rows_in
+    pack = proj_send.shape[1]
+    per_row = heads // rows_in
+    head_dim = LANES // per_row
+    group_rows = rows_in // rows_map
+
+    my_kv = lax.axis_index("kv")
+    my_tp = lax.axis_index("tp")
+    me = my_kv * tp + my_tp
+
+    if kv == 4:
+        half = my_kv // 2
+        chips = [my_kv + 1 - 2 * lax.rem(my_kv, 2), 2 - half, 3 - 3 * half]
+    else:
+        chips = [lax.rem(my_kv + d, kv) for d in range(1, kv)]
+    peers = []
+    for pk, first_t in [(pk, 0) for pk in reversed(chips)] + [(my_kv, 1)]:
+        for t in range(first_t, tp):
+            pt = lax.rem(my_tp + t, tp)
+            peers.append((pk * tp + pt, {"kv": pk, "tp": pt}))
+
+    loads = {}
+
+    def load(name, src, dst):
+        copy = pltpu.make_async_copy(src, dst, load_sem.at[len(loads)])
+        copy.start()
+        loads[name] = copy
+
+    def ready(*names):
+        for name in names:
+            loads[name].wait()
+
+    sends = []
+
+    def send(phase, index, src, dst):
+        peer, where = peers[index]
+        copy = pltpu.make_async_remote_copy(
+            src_ref=src,
+            dst_ref=dst,
+            send_sem=send_sem.at[phase, index],
+            recv_sem=recv_sem.at[phase, me],
+            device_id=where,
+            device_id_type=MESH,
+        )
+        copy.start()
+        sends.append(copy)
+
+    def arrive(phase, index, dst):
+        peer, where = peers[index]
+        pltpu.make_async_remote_copy(
+            src_ref=dst,
+            dst_ref=dst,
+            send_sem=send_sem.at[phase, index],
+            recv_sem=recv_sem.at[phase, peer],
+            device_id=where,
+            device_id_type=MESH,
+        ).wait_recv()
+
+    barrier = pltpu.get_barrier_semaphore()
+    for _, where in peers:
+        pl.semaphore_signal(barrier, inc=1, device_id=where, device_id_type=MESH)
+    load("tokens", tokens, tok_all.at[me])
+    load("g1", first_gain, g1)
+    load("wg1", first_gate, wg1)
+    load("wu1", first_up, wu1)
+    load("wd1", first_down, wd1)
+    load("mg", mix_gain, mg)
+    load("hist", conv_history.at[0], hist)
+    load("taps", conv_taps, taps)
+    load("bias", step_bias, bias)
+    load("rate", rate_log, rate)
+    load("ggain", group_gain, ggain)
+    load("g2", second_gain, g2)
+    ready("tokens")
+    pl.semaphore_wait(barrier, n - 1)
+    for i in range(n - 1):
+        send(0, i, tok_all.at[me], tok_all.at[me])
+    load("wi", w_input, wi)
+    load("ww", w_write, ww)
+    load("wr", w_read, wr)
+    load("wo", w_outgate, wo)
+    load("ws", w_step, ws)
+    load("state", mixer_state, state)
+
+    ready("hist", "taps")
+    for k in range(rows_conv):
+        lanes = slice(k * LANES, (k + 1) * LANES)
+        hist_f[:, k, :] = hist[:, lanes].astype(F32)
+        taps_f[:, k, :] = taps[:, lanes].astype(F32)
+
+    def half_block(phase, slots, gain, w_gate, w_up, w_down, names, down_send, down_recv, fill):
+        ready(*names[:3])
+        block = tp * chan
+        power = gate = upper = None
+        for c, pk in enumerate([my_kv] + chips):
+            size = tp - 1 if c == 0 else tp
+            start = len(peers) - (tp - 1) - c * tp
+            for i in range(start, start + size):
+                arrive(phase, i, slots.at[peers[i][0]])
+            resid = jnp.concatenate([slots[pk * tp + t] for t in range(tp)], axis=1).astype(F32)
+            columns = pl.ds(pl.multiple_of(pk * block, block), block)
+            weighted = (resid * gain[:, columns]).astype(BF16)
+            terms = (
+                resid * resid,
+                dot_rows(weighted, w_gate[:, columns]),
+                dot_rows(weighted, w_up[:, columns]),
+            )
+            if c == 0:
+                power, gate, upper = terms
+            else:
+                power, gate, upper = power + terms[0], gate + terms[1], upper + terms[2]
+        scale = lax.rsqrt(jnp.sum(power, axis=1, keepdims=True) / width + EPS)
+        hidden = (silu(gate * scale) * (upper * scale)).astype(BF16)
+        ready(names[3])
+
+        def part(dest):
+            columns = pl.ds(pl.multiple_of(dest * chan, chan), chan)
+            return jnp.dot(hidden, w_down[:, columns], preferred_element_type=F32)
+
+        for i, (peer, _) in enumerate(peers):
+            down_send[i] = part(peer).astype(BF16)
+            send(phase + 1, i, down_send.at[i], down_recv.at[me])
+        total = part(me)
+        fill()
+        for i in reversed(range(n - 1)):
+            peer = peers[i][0]
+            arrive(phase + 1, i, down_recv.at[peer])
+            total = total + down_recv[peer].astype(F32)
+        own = slots[me].astype(F32)
+        return (own + 0.5 * total).astype(BF16)
+
+    load("wout", w_output, wout)
+    load("wg2", second_gate, wg2)
+    load("wu2", second_up, wu2)
+    load("wd2", second_down, wd2)
+
+    def round_state():
+        ready("state")
+        state_b[...] = state[...].astype(BF16)
+
+    first = half_block(
+        0,
+        tok_all,
+        g1,
+        wg1,
+        wu1,
+        wd1,
+        ("g1", "wg1", "wu1", "wd1"),
+        down_send1,
+        down_recv1,
+        round_state,
+    )
+    first_f = first.astype(F32)
+
+    ready("mg", "wi", "ww", "wr", "wo", "ws")
+    squares = jnp.sum(first_f * first_f, axis=1, keepdims=True)
+    premix = (first_f * mg[...]).astype(BF16)
+    row = 0
+    for weight in (wi, ww, wr, wo):
+        part = jnp.dot(premix, weight[...], preferred_element_type=F32)
+        for k in range(weight.shape[1] // LANES):
+            proj_f[:, row, :] = part[:, k * LANES : (k + 1) * LANES]
+            row += 1
+    step_f[...] = jnp.zeros_like(step_f)
+    step_f[:, :heads] = dot_rows(premix, ws[...])
+    high = squares.astype(BF16).astype(F32)
+    lane = lax.broadcasted_iota(jnp.int32, (rows, LANES), 1)
+    last = jnp.where(lane == heads, high, step_f[...])
+    last = jnp.where(lane == heads + 1, squares - high, last)
+    proj_f[:, row, :] = last
+    for k in range(row + 1, pack):
+        proj_f[:, k, :] = jnp.zeros((rows, LANES), F32)
+    for i, (peer, _) in enumerate(peers):
+        proj_send[i] = proj_f[peer].astype(BF16)
+        send(2, i, proj_send.at[i], proj_recv.at[me])
+    summed = proj_f[me]
+    for i in reversed(range(n - 1)):
+        peer = peers[i][0]
+        arrive(2, i, proj_recv.at[peer])
+        summed = summed + proj_recv[peer].astype(F32)
+
+    tail = summed[rows_all : rows_all + 1]
+    own_squares = tail[:, heads : heads + 1] + tail[:, heads + 1 : heads + 2]
+    scale = lax.rsqrt(own_squares / width + EPS)
+    scaled = (scale * summed).astype(BF16).astype(F32)
+    fresh = scaled[:rows_conv]
+    conv = taps_f[3] * fresh
+    for k in range(3):
+        conv = conv + taps_f[k] * hist_f[k]
+    conv = silu(conv)
+    conv_in = conv[:rows_in]
+    conv_write = conv[rows_in : rows_in + rows_map]
+    conv_read = conv[rows_in + rows_map :]
+    outgate = scaled[rows_conv:rows_all]
+
+    ready("bias", "rate", "ggain")
+    steps_raw = scaled[rows_all : rows_all + 1, :heads] + bias[...]
+    step_row = jnp.maximum(steps_raw, 0.0) + jnp.log1p(jnp.exp(-jnp.abs(steps_raw)))
+    decay_row = jnp.exp(-step_row * jnp.exp(rate[...]))
+    r_id = lax.broadcasted_iota(jnp.int32, (rows_in, heads), 0)
+    h_id = lax.broadcasted_iota(jnp.int32, (rows_in, heads), 1)
+    wide_lane = lax.broadcasted_iota(jnp.int32, (rows_in, LANES), 1)
+
+    def spread(values):
+        out = jnp.zeros((rows_in, LANES), F32)
+        for k in range(per_row):
+            mine = jnp.where(h_id == r_id * per_row + k, values, 0.0)
+            column = jnp.sum(mine, axis=1, keepdims=True)
+            inside = (wide_lane >= k * head_dim) & (wide_lane < (k + 1) * head_dim)
+            out = jnp.where(inside, column, out)
+        return out
+
+    step_c = spread(step_row)
+    decay_c = spread(decay_row)
+    fed = step_c * conv_in
+
+    read_high = conv_read.astype(BF16).astype(F32)
+    lhs = jnp.concatenate([read_high, conv_read - read_high], axis=0).astype(BF16)
+    dots = dot_rows(lhs, state_b[...])
+    pieces = []
+    for r in range(rows_in):
+        g = r // group_rows
+        lanes = slice(r * LANES, (r + 1) * LANES)
+        pieces.append(dots[g : g + 1, lanes] + dots[rows_map + g : rows_map + g + 1, lanes])
+    old_read = jnp.concatenate(pieces, axis=0)
+    both = jnp.sum(conv_write * conv_read, axis=1, keepdims=True)
+    both = jnp.concatenate(
+        [jnp.broadcast_to(both[g : g + 1], (group_rows, 1)) for g in range(rows_map)], axis=0
+    )
+    read_out = decay_c * old_read + fed * both
+    gated = read_out * silu(outgate)
+    power = jnp.sum(gated * gated, axis=1, keepdims=True)
+    power = jnp.concatenate(
+        [
+            jnp.broadcast_to(
+                jnp.sum(power[g * group_rows : (g + 1) * group_rows], axis=0, keepdims=True),
+                (group_rows, 1),
+            )
+            for g in range(rows_map)
+        ],
+        axis=0,
+    )
+    block_scale = lax.rsqrt(power / (group_rows * LANES) + EPS)
+    norm_all[me] = (gated * block_scale * ggain[...]).astype(BF16)
+    for i in range(n - 1):
+        send(3, i, norm_all.at[me], norm_all.at[me])
+
+    decay_t = jnp.transpose(decay_c)
+    fed_t = jnp.transpose(fed)
+    for r in range(rows_in):
+        g = r // group_rows
+        block = slice(r * LANES, (r + 1) * LANES)
+        state_out[block] = (
+            decay_t[:, r : r + 1] * state[block]
+            + fed_t[:, r : r + 1] * conv_write[g : g + 1]
+        )
+    fresh_f[...] = fresh
+    kept = hist.shape[0]
+    tail_f[0 : kept - 1, :] = hist[...].astype(F32)[1:]
+    for k in range(rows_conv):
+        tail_f[kept - 1 : kept, k * LANES : (k + 1) * LANES] = fresh_f[k : k + 1, :]
+    history_out[...] = tail_f[...].astype(BF16)
+
+    for i in reversed(range(n - 1)):
+        arrive(3, i, norm_all.at[peers[i][0]])
+    for j in range(n):
+        norm_f[j] = norm_all[j].astype(F32)
+    normed = jnp.concatenate([norm_f[:, r, :] for r in range(rows_in)], axis=1).astype(BF16)
+    ready("wout")
+    mixed = jnp.dot(normed, wout[...], preferred_element_type=F32)
+    sec_all[me] = (first_f + mixed).astype(BF16)
+    for i in range(n - 1):
+        send(4, i, sec_all.at[me], sec_all.at[me])
+    layer_out[...] = half_block(
+        4,
+        sec_all,
+        g2,
+        wg2,
+        wu2,
+        wd2,
+        ("g2", "wg2", "wu2", "wd2"),
+        down_send2,
+        down_recv2,
+        lambda: None,
+    )
+    for copy in sends:
+        copy.wait_send()
+
+
+def write_kernel(layer_in, state_in, history_in, layer_out, state_out, history_out, sem):
+    copies = [
+        pltpu.make_async_copy(state_in, state_out, sem.at[0]),
+        pltpu.make_async_copy(layer_in, layer_out, sem.at[1]),
+        pltpu.make_async_copy(history_in, history_out.at[0], sem.at[2]),
+    ]
+    for copy in copies:
+        copy.start()
+    for copy in copies:
+        copy.wait()
+
+
+NAMES = (
+    "tokens",
+    "first_gain",
+    "first_gate",
+    "first_up",
+    "first_down",
+    "mix_gain",
+    "w_input",
+    "w_outgate",
+    "w_write",
+    "w_read",
+    "w_step",
+    "conv_taps",
+    "conv_history",
+    "step_bias",
+    "rate_log",
+    "mixer_state",
+    "group_gain",
+    "w_output",
+    "second_gain",
+    "second_gate",
+    "second_up",
+    "second_down",
+)
+
+
+def fused_body(kv, tp, *args):
+    a = dict(zip(NAMES, args))
+    n = kv * tp
+    rows, chan = a["tokens"].shape
+    state_shape = a["mixer_state"].shape
+    heads = state_shape[1]
+    hist_shape = a["conv_history"].shape
+    for name in ("first_gain", "mix_gain", "second_gain", "step_bias", "rate_log"):
+        a[name] = a[name].reshape(1, -1)
+    for name in ("first_gate", "first_up", "w_step", "second_gate", "second_up"):
+        a[name] = a[name].T
+    a["group_gain"] = a["group_gain"].reshape(-1, LANES)
+    a["mixer_state"] = a["mixer_state"].reshape(-1, state_shape[3])
+    rows_in = a["w_input"].shape[1] // LANES
+    rows_conv = hist_shape[2] // LANES
+    pack = -(-(rows_conv + rows_in + 1) // 16) * 16
+
+    def held(name):
+        return pltpu.VMEM(a[name].shape, a[name].dtype)
+
+    in_hbm = pl.BlockSpec(memory_space=pltpu.HBM)
+    in_vmem = pl.BlockSpec(memory_space=pltpu.VMEM)
+    shapes = (
+        ((rows, chan), BF16),
+        (a["mixer_state"].shape, F32),
+        (hist_shape[1:], BF16),
+    )
+    kept_bytes = sum(math.prod(shape) * jnp.dtype(kind).itemsize for shape, kind in shapes)
+    kept_bytes += 64 * 1024
+    out = pl.pallas_call(
+        functools.partial(layer_kernel, kv, tp, heads),
+        out_shape=tuple(pltpu.VMEM(*shape) for shape in shapes),
+        in_specs=[in_hbm] * len(NAMES),
+        out_specs=(in_vmem,) * 3,
+        scratch_shapes=[
+            held("first_gain"),
+            held("first_gate"),
+            held("first_up"),
+            held("first_down"),
+            held("mix_gain"),
+            held("w_input"),
+            held("w_outgate"),
+            held("w_write"),
+            held("w_read"),
+            held("w_step"),
+            held("conv_taps"),
+            pltpu.VMEM(hist_shape[1:], BF16),
+            held("step_bias"),
+            held("rate_log"),
+            held("mixer_state"),
+            held("group_gain"),
+            held("w_output"),
+            held("second_gain"),
+            held("second_gate"),
+            held("second_up"),
+            held("second_down"),
+            pltpu.VMEM((n, rows, chan), BF16),
+            pltpu.VMEM((n - 1, rows, chan), BF16),
+            pltpu.VMEM((n, rows, chan), BF16),
+            pltpu.VMEM((n - 1, pack, LANES), BF16),
+            pltpu.VMEM((n, pack, LANES), BF16),
+            pltpu.VMEM((n, rows_in, LANES), BF16),
+            pltpu.VMEM((n, rows, chan), BF16),
+            pltpu.VMEM((n - 1, rows, chan), BF16),
+            pltpu.VMEM((n, rows, chan), BF16),
+            pltpu.VMEM((rows, pack, LANES), F32),
+            pltpu.VMEM((rows, LANES), F32),
+            pltpu.VMEM(a["mixer_state"].shape, BF16),
+            pltpu.VMEM((hist_shape[1], rows_conv, LANES), F32),
+            pltpu.VMEM((hist_shape[1] + 1, rows_conv, LANES), F32),
+            pltpu.VMEM((rows_conv, LANES), F32),
+            pltpu.VMEM((rows, LANES), F32),
+            pltpu.VMEM(hist_shape[1:], F32),
+            pltpu.VMEM((n, rows_in, LANES), F32),
+            pltpu.SemaphoreType.DMA((len(NAMES),)),
+            pltpu.SemaphoreType.DMA((6, n - 1)),
+            pltpu.SemaphoreType.DMA((6, n)),
+        ],
+        compiler_params=pltpu.CompilerParams(
+            collective_id=0, has_side_effects=True, vmem_limit_bytes=VMEM_BYTES - kept_bytes
+        ),
+        name="layer",
+    )(*(a[name] for name in NAMES))
+    layer_out, state_out, history_out = pl.pallas_call(
+        write_kernel,
+        out_shape=(
+            jax.ShapeDtypeStruct((rows, chan), BF16),
+            jax.ShapeDtypeStruct(a["mixer_state"].shape, F32),
+            jax.ShapeDtypeStruct(hist_shape, BF16),
+        ),
+        in_specs=[in_vmem] * 3,
+        out_specs=(in_hbm,) * 3,
+        scratch_shapes=[pltpu.SemaphoreType.DMA((3,))],
+        compiler_params=pltpu.CompilerParams(vmem_limit_bytes=4 * 1024 * 1024),
+        name="write",
+    )(*out)
+    return layer_out, state_out.reshape(state_shape), history_out
+
+
+def half_block_parts(resid, gain, w_gate, w_up, w_down):
     whole = lax.all_gather(resid, ("kv", "tp"), axis=1, tiled=True)
     whole_f = whole.astype(jnp.float32)
     scale = lax.rsqrt(jnp.mean(whole_f * whole_f, axis=-1, keepdims=True) + EPS)
@@ -51,7 +574,7 @@
     ssd_width = heads * head_dim
     groups = w_write.shape[1] // state_dim
     per_group = heads // groups
-    first = half_block(tokens, first_gain, first_gate, first_up, first_down)
+    first = half_block_parts(tokens, first_gain, first_gate, first_up, first_down)
     first_f = first.astype(jnp.float32)
     squares = jnp.sum(first_f * first_f, axis=1)
     premix = (first_f * mix_gain).astype(jnp.bfloat16)
@@ -104,14 +627,35 @@
         preferred_element_type=jnp.float32,
     )
     second = (first_f + mixed).astype(jnp.bfloat16)
-    layer_out = half_block(second, second_gain, second_gate, second_up, second_down)
+    layer_out = half_block_parts(second, second_gain, second_gate, second_up, second_down)
     state_out = new_state.reshape(count, heads, head_dim, state_dim)
     return (layer_out, state_out, history_out)
 
 
+def run_body(kv, tp, *args):
+    tokens, state, taps = args[0], args[15], args[11]
+    w_input, w_write = args[6], args[8]
+    rows, chan = tokens.shape
+    count, heads, head_dim, state_dim = state.shape
+    fits = (
+        count == 1
+        and rows == kv * tp
+        and rows == 8
+        and chan % LANES == 0
+        and state_dim == LANES
+        and LANES % head_dim == 0
+        and taps.shape[0] == 4
+        and heads + 2 <= LANES
+        and (w_input.shape[1] // LANES) % (w_write.shape[1] // LANES) == 0
+    )
+    if fits:
+        return fused_body(kv, tp, *args)
+    return body(*args)
+
+
 def solution(mesh):
     return jax.shard_map(
-        body,
+        functools.partial(run_body, mesh.shape["kv"], mesh.shape["tp"]),
         mesh=mesh,
         in_specs=(
             P("dp", ("kv", "tp")),

time: 235 us -> 32.9 us (0.14)
  waiting for transfers between devices: 110 us -> 0 us
  blocking collectives: 70.6 us -> 0 us
  Pallas kernels: 0 us -> 32.1 us
  matrix products: 24.4 us -> 0 us
  between operations: 14.7 us -> 0.65 us
  other arithmetic: 11.7 us -> 0 us
    reduce_scatter x2 -> x0, waiting for transfers between devices: 57.2 us -> none  [half_block(): lax.psum_scatter(down, ('kv', 'tp'), scatter_dimension=1, tiled=True)]
    unnamed x4 -> x0, waiting for transfers between devices: 53 us -> none
    all_gather x3 -> x0, blocking collectives: 44.2 us -> none  [the longest x2 30.1 us: half_block(): whole = lax.all_gather(resid, ('kv', 'tp'), axis=1, tiled=True)]
    pallas_call x0 -> x2, Pallas kernels: none -> 32.1 us  [the longest x1 31.1 us: fused_body(): pl.pallas_call(functools.partial(layer_kernel, kv, tp, heads), out_shape=...]
    unnamed x1 -> x0, blocking collectives: 26.4 us -> none
    dot_general x11 -> x0, matrix products: 24.4 us -> none  [the longest x2 9.15 us: half_block(): down = jnp.dot(hidden, w_down, preferred_element_type=jnp.float32)]
    convert_element_type x4 -> x0, other arithmetic: 3.45 us -> none  [the longest x1 1.5 us: body(): inputs = (scale * summed[0]).astype(jnp.bfloat16)]
    add x1 -> x0, other arithmetic: 2.59 us -> none  [body(): new_state = decay_g[..., None, None] * state + written]
  transfers between devices with their start and end apart: 3 -> 0, of which waited for: 3 -> 0; matrix products, arithmetic and copies ran while one was open for 2% -> 0% of each run, Pallas kernels for 0% -> 0%
where the time goes in v1:
time: 32.9 us; the launch traced here: 32.7 us
  Pallas kernels  32.1 us (98%)
  between operations  0.65 us (2%)
    pallas_call x1, Pallas kernels, fused_body(): pl.pallas_call(functools.partial(layer_kernel, kv, tp, heads), out_shape=...  31.1 us
    pallas_call x1, Pallas kernels, fused_body(): pl.pallas_call(write_kernel, out_shape=(jax.ShapeDtypeStruct((rows, chan)...  1 us

profile of v1, /device:TPU:0, one launch (start us, length us, event | category | flops | bytes accessed | tf_op | source)
XLA Modules:
  0.0 32.7 jit_solution(9637935904769086616)
XLA Ops:
  0.6 31.1 %layer.1 = (bf16[8,256]{1,0:T(8,128)(2,1)S(1)}, f32[2048,128]{1,0:T(8,128)S(1)}, bf16[3,3072]{1,0:T(4,128)(2,1)S(1)}) custom-call(bf16[8,256]{1,0:T(8,128)(2,1)} %tokens.1, f32[1,2048]{1,0:T(1,128)} %bitcast.19, bf16[704,2048]{1,0:T(8,128)(2,1)} %bitcast.13, bf16[704,2048]{1,0:T(8,128)(2,1)} %bitcast.14, bf16[704,2048]{1,0:T(8,128)(2,1)} %first_down.1, ...), custom_call_target="tpu_custom_call" | custom-call | tf_op jit(solution)/shard_map/layer/pallas_call | solution.py:462
  31.7 1.0 %write.1 = (bf16[8,256]{1,0:T(8,128)(2,1)}, f32[2048,128]{1,0:T(8,128)}, bf16[1,3,3072]{2,1,0:T(4,128)(2,1)}) custom-call(bf16[8,256]{1,0:T(8,128)(2,1)S(1)} %get-tuple-element.9.layer_in, f32[2048,128]{1,0:T(8,128)S(1)} %get-tuple-element.10.state_in, bf16[3,3072]{1,0:T(4,128)(2,1)S(1)} %get-tuple-element.11.history_in), custom_call_target="tpu_custom_call" | custom-call | tf_op jit(solution)/shard_map/write/pallas_call | solution.py:516

commit v2 on v1

--- a/solution.py
+++ b/solution.py
@@ -119,10 +119,12 @@
     else:
         chips = [lax.rem(my_kv + d, kv) for d in range(1, kv)]
     peers = []
-    for pk, first_t in [(pk, 0) for pk in reversed(chips)] + [(my_kv, 1)]:
-        for t in range(first_t, tp):
-            pt = lax.rem(my_tp + t, tp)
-            peers.append((pk * tp + pt, {"kv": pk, "tp": pt}))
+    for pk in reversed(chips):
+        for t in range(tp):
+            peers.append((pk * tp + t, {"kv": pk, "tp": t}))
+    for t in range(1, tp):
+        pt = lax.rem(my_tp + t, tp)
+        peers.append((my_kv * tp + pt, {"kv": my_kv, "tp": pt}))
 
     loads = {}
 
@@ -166,12 +168,12 @@
         pl.semaphore_signal(barrier, inc=1, device_id=where, device_id_type=MESH)
     load("tokens", tokens, tok_all.at[me])
     load("g1", first_gain, g1)
+    load("hist", conv_history.at[0], hist)
+    load("taps", conv_taps, taps)
     load("wg1", first_gate, wg1)
     load("wu1", first_up, wu1)
     load("wd1", first_down, wd1)
     load("mg", mix_gain, mg)
-    load("hist", conv_history.at[0], hist)
-    load("taps", conv_taps, taps)
     load("bias", step_bias, bias)
     load("rate", rate_log, rate)
     load("ggain", group_gain, ggain)
@@ -197,24 +199,25 @@
         ready(*names[:3])
         block = tp * chan
         power = gate = upper = None
-        for c, pk in enumerate([my_kv] + chips):
-            size = tp - 1 if c == 0 else tp
-            start = len(peers) - (tp - 1) - c * tp
-            for i in range(start, start + size):
-                arrive(phase, i, slots.at[peers[i][0]])
-            resid = jnp.concatenate([slots[pk * tp + t] for t in range(tp)], axis=1).astype(F32)
-            columns = pl.ds(pl.multiple_of(pk * block, block), block)
+        steps = [[(None, me)]] + [[(i, peers[i][0])] for i in reversed(range(n - 1))]
+        for step in steps:
+            for i, owner in step:
+                if i is not None:
+                    arrive(phase, i, slots.at[owner])
+            resid = jnp.concatenate([slots[owner] for _, owner in step], axis=1).astype(F32)
+            start = pl.multiple_of(step[0][1] * chan, chan)
+            columns = pl.ds(start, len(step) * chan)
             weighted = (resid * gain[:, columns]).astype(BF16)
             terms = (
-                resid * resid,
+                jnp.sum(resid * resid, axis=1, keepdims=True),
                 dot_rows(weighted, w_gate[:, columns]),
                 dot_rows(weighted, w_up[:, columns]),
             )
-            if c == 0:
+            if power is None:
                 power, gate, upper = terms
             else:
                 power, gate, upper = power + terms[0], gate + terms[1], upper + terms[2]
-        scale = lax.rsqrt(jnp.sum(power, axis=1, keepdims=True) / width + EPS)
+        scale = lax.rsqrt(power / width + EPS)
         hidden = (silu(gate * scale) * (upper * scale)).astype(BF16)
         ready(names[3])
 
@@ -222,8 +225,15 @@
             columns = pl.ds(pl.multiple_of(dest * chan, chan), chan)
             return jnp.dot(hidden, w_down[:, columns], preferred_element_type=F32)
 
-        for i, (peer, _) in enumerate(peers):
-            down_send[i] = part(peer).astype(BF16)
+        for c, pk in enumerate(reversed(chips)):
+            columns = pl.ds(pl.multiple_of(pk * block, block), block)
+            wide = jnp.dot(hidden, w_down[:, columns], preferred_element_type=F32).astype(BF16)
+            for t in range(tp):
+                i = c * tp + t
+                down_send[i] = wide[:, t * chan : (t + 1) * chan]
+                send(phase + 1, i, down_send.at[i], down_recv.at[me])
+        for i in range(len(chips) * tp, n - 1):
+            down_send[i] = part(peers[i][0]).astype(BF16)
             send(phase + 1, i, down_send.at[i], down_recv.at[me])
         total = part(me)
         fill()
@@ -241,7 +251,9 @@
 
     def round_state():
         ready("state")
-        state_b[...] = state[...].astype(BF16)
+        for r in range(rows_in):
+            block = slice(r * LANES, (r + 1) * LANES)
+            state_b[:, block] = jnp.transpose(state[block]).astype(BF16)
 
     first = half_block(
         0,
@@ -321,7 +333,7 @@
 
     read_high = conv_read.astype(BF16).astype(F32)
     lhs = jnp.concatenate([read_high, conv_read - read_high], axis=0).astype(BF16)
-    dots = dot_rows(lhs, state_b[...])
+    dots = jnp.dot(lhs, state_b[...], preferred_element_type=F32)
     pieces = []
     for r in range(rows_in):
         g = r // group_rows
@@ -497,7 +509,7 @@
             pltpu.VMEM((n, rows, chan), BF16),
             pltpu.VMEM((rows, pack, LANES), F32),
             pltpu.VMEM((rows, LANES), F32),
-            pltpu.VMEM(a["mixer_state"].shape, BF16),
+            pltpu.VMEM(a["mixer_state"].shape[::-1], BF16),
             pltpu.VMEM((hist_shape[1], rows_conv, LANES), F32),
             pltpu.VMEM((hist_shape[1] + 1, rows_conv, LANES), F32),
             pltpu.VMEM((rows_conv, LANES), F32),

time: 32.9 us -> 31.7 us (0.964)
  Pallas kernels: 32.1 us -> 30.9 us
    pallas_call x1, Pallas kernels: 31.1 us -> 29.9 us  [fused_body(): pl.pallas_call(functools.partial(layer_kernel, kv, tp, heads), out_shape=...]
where the time goes in v2:
time: 31.7 us; the launch traced here: 31.6 us
  Pallas kernels  30.9 us (97%)
  between operations  0.65 us (2%)
    pallas_call x1, Pallas kernels, fused_body(): pl.pallas_call(functools.partial(layer_kernel, kv, tp, heads), out_shape=...  29.9 us
    pallas_call x1, Pallas kernels, fused_body(): pl.pallas_call(write_kernel, out_shape=(jax.ShapeDtypeStruct((rows, chan)...  1 us

profile of v2, /device:TPU:0, one launch (start us, length us, event | category | flops | bytes accessed | tf_op | source)
XLA Modules:
  0.0 31.6 jit_solution(2451961300451152482)
XLA Ops:
  0.6 29.9 %layer.1 = (bf16[8,256]{1,0:T(8,128)(2,1)S(1)}, f32[2048,128]{1,0:T(8,128)S(1)}, bf16[3,3072]{1,0:T(4,128)(2,1)S(1)}) custom-call(bf16[8,256]{1,0:T(8,128)(2,1)} %tokens.1, f32[1,2048]{1,0:T(1,128)} %bitcast.19, bf16[704,2048]{1,0:T(8,128)(2,1)} %bitcast.13, bf16[704,2048]{1,0:T(8,128)(2,1)} %bitcast.14, bf16[704,2048]{1,0:T(8,128)(2,1)} %first_down.1, ...), custom_call_target="tpu_custom_call" | custom-call | tf_op jit(solution)/shard_map/layer/pallas_call | solution.py:474
  30.5 1.0 %write.1 = (bf16[8,256]{1,0:T(8,128)(2,1)}, f32[2048,128]{1,0:T(8,128)}, bf16[1,3,3072]{2,1,0:T(4,128)(2,1)}) custom-call(bf16[8,256]{1,0:T(8,128)(2,1)S(1)} %get-tuple-element.9.layer_in, f32[2048,128]{1,0:T(8,128)S(1)} %get-tuple-element.10.state_in, bf16[3,3072]{1,0:T(4,128)(2,1)S(1)} %get-tuple-element.11.history_in), custom_call_target="tpu_custom_call" | custom-call | tf_op jit(solution)/shard_map/write/pallas_call | solution.py:528
